TPU v7x, 32 devices: a whole 2x2x4 slice. The times are simulated.
32 devices in a mesh: tp: 32 (over z, y, x, core).
Axes of the slice: x: 2, y: 2, z: 4, core: 2. Of those that a mesh axis runs over, the one named last changes fastest.
Arguments:
- tokens: bfloat16 [4096, 256], P('tp'), may hold values from -20 to 20, as said below
- positions: int32 [256], replicated, may hold values from 1 to 3072, 262144 in all
- norm_gain: float32 [4096], replicated, may hold values from 0.1 to 1.9
- w_query: bfloat16 [1024, 4096], P('tp'), may hold values from -0.09375 to 0.09375
- w_key: bfloat16 [1024, 4096], P('tp'), may hold values from -0.09375 to 0.09375
- w_value: bfloat16 [2048, 4096], P('tp'), may hold values from -0.09375 to 0.09375
- w_outgate: bfloat16 [2048, 4096], P('tp'), may hold values from -0.09375 to 0.09375
- w_input: bfloat16 [4, 4096], replicated, may hold values from -0.09375 to 0.09375
- w_forget: bfloat16 [4, 4096], replicated, may hold values from -0.09375 to 0.09375
- bias_input: float32 [4], replicated, may hold values from -3 to 3
- bias_forget: float32 [4], replicated, may hold values from -1 to 4
- w_read: bfloat16 [4096, 2048], P('tp'), may hold values from -0.125 to 0.125
- cells: float32 [2048, 256, 256], P('tp'), may hold values from -4 to 4
- norms: float32 [1024, 256], replicated, may hold values from 0 to 0.5
- maxima: float32 [4, 256], replicated, may hold values from -1 to 1
Outputs:
- mixed_rows: bfloat16 [4096, 256], P('tp')
- new_cells: float32 [2048, 256, 256], P('tp')
- new_norms: float32 [1024, 256], replicated
- new_maxima: float32 [4, 256], replicated
Inputs may be any that keep to these rules, and one draw needn't show every extreme that they name: `tokens`: feature rows have their own scales, spread over a factor of ten.
All inputs are finite; a program needn't handle non-finite values.
Results may differ from a plain program's by a relative error of at most 0.0062.
The roundings to bfloat16 on the way count: a program that leaves them out, or rounds other values in their place, can miss the bound.
Values may be sent and summed in bfloat16 or wider, within the bound.
A program may use at most 128 MiB of HBM per device.

v0:
```python
import jax
import jax.numpy as jnp
from jax import lax
from jax.sharding import PartitionSpec as P

DQK = 256
MOST_LEN = 3072


EPS = 1e-06


def mix_block(
    rows,
    where,
    gain,
    w_query,
    w_key,
    w_value,
    w_outgate,
    w_input,
    w_forget,
    bias_input,
    bias_forget,
    w_read,
    cells,
    norms,
    maxima,
):
    count = lax.axis_size("tp")
    index = lax.axis_index("tp")
    seqs = rows.shape[1]
    model_width = gain.shape[0]
    heads = w_input.shape[0]
    head = index * heads // count
    whole = lax.all_gather(rows, "tp", axis=0, tiled=True).astype(jnp.float32)
    total = jnp.sum(whole * whole, axis=0)
    normed = (whole * gain[:, None]).astype(jnp.bfloat16)
    scale = lax.rsqrt(total / model_width + EPS)[None, :]
    query_loc = (jnp.dot(w_query, normed, preferred_element_type=jnp.float32) * scale).astype(
        jnp.bfloat16
    )
    key_loc = (
        jnp.dot(w_key, normed, preferred_element_type=jnp.float32) * scale * DQK ** (-0.5)
    ).astype(jnp.bfloat16)
    query_all, key_all = (
        lax.all_gather(query_loc, "tp", axis=0, tiled=True),
        lax.all_gather(key_loc, "tp", axis=0, tiled=True),
    )
    value = jnp.dot(w_value, normed, preferred_element_type=jnp.float32) * scale
    outgate = jnp.dot(w_outgate, normed, preferred_element_type=jnp.float32) * scale
    gate_in = (
        jnp.dot(w_input, normed, preferred_element_type=jnp.float32) * scale + bias_input[:, None]
    )
    gate_forget = (
        jnp.dot(w_forget, normed, preferred_element_type=jnp.float32) * scale + bias_forget[:, None]
    )
    logf = jax.nn.log_sigmoid(gate_forget) * (1.0 + where / MOST_LEN)
    new_max = jnp.maximum(logf + maxima, gate_in)
    decay = jnp.exp(logf + maxima - new_max)
    fresh = jnp.exp(gate_in - new_max)
    queries = query_all.astype(jnp.float32).reshape(heads, DQK, seqs)
    keys = key_all.astype(jnp.float32).reshape(heads, DQK, seqs)
    norms_new = decay[:, None, :] * norms.reshape(heads, DQK, seqs) + fresh[:, None, :] * keys
    denom = jnp.sum(queries * norms_new, axis=1)
    decay_own = lax.dynamic_index_in_dim(decay, head, 0)
    fresh_own = lax.dynamic_index_in_dim(fresh, head, 0)
    den_own = lax.dynamic_index_in_dim(denom, head, 0)
    q_head = lax.dynamic_slice_in_dim(query_all, head * DQK, DQK, 0).astype(jnp.float32)
    k_head = lax.dynamic_slice_in_dim(key_all, head * DQK, DQK, 0).astype(jnp.float32)
    new_cells = decay_own[None] * cells + fresh_own[None] * value[:, None, :] * k_head[None, :, :]
    numer = jnp.sum(q_head[None, :, :] * new_cells, axis=1)
    hidden = numer / jnp.maximum(jnp.abs(den_own), 1.0)
    gated = (hidden * jax.nn.sigmoid(outgate)).astype(jnp.bfloat16)
    mixed = jnp.dot(
        w_read, lax.all_gather(gated, "tp", axis=0, tiled=True), preferred_element_type=jnp.float32
    )
    new_rows = (rows.astype(jnp.float32) + mixed).astype(jnp.bfloat16)
    return (new_rows, new_cells, norms_new.reshape(heads * DQK, seqs), new_max)


def shards(
    tokens,
    positions,
    norm_gain,
    w_query,
    w_key,
    w_value,
    w_outgate,
    w_input,
    w_forget,
    bias_input,
    bias_forget,
    w_read,
    cells,
    norms,
    maxima,
):
    row_parts, cell_parts, norm_parts, max_parts = ([], [], [], [])
    where = positions.astype(jnp.float32)[None, :]
    rows, cell_new, norm_new, max_new = mix_block(
        tokens,
        where,
        norm_gain,
        w_query,
        w_key,
        w_value,
        w_outgate,
        w_input,
        w_forget,
        bias_input,
        bias_forget,
        w_read,
        cells,
        norms,
        maxima,
    )
    row_parts.append(rows)
    cell_parts.append(cell_new)
    norm_parts.append(norm_new)
    max_parts.append(max_new)
    return (row_parts[0], cell_parts[0], norm_parts[0], max_parts[0])


def solution(mesh):
    return jax.shard_map(
        shards,
        mesh=mesh,
        in_specs=(
            P("tp", None),
            P(),
            P(),
            P("tp", None),
            P("tp", None),
            P("tp", None),
            P("tp", None),
            P(),
            P(),
            P(),
            P(),
            P("tp", None),
            P("tp", None, None),
            P(),
            P(),
        ),
        out_specs=(P("tp", None), P("tp", None, None), P(), P()),
        check_vma=False,
    )
```

profile of v0, /device:TPU:1, one launch (start us, length us, event | category | flops | bytes accessed | tf_op | source)
XLA Modules:
  0.0 224.9 jit_solution(209790742537551208)
XLA Ops:
  7.2 0.0 all-gather.3.cloned.1.call-start
  7.2 0.7 all-gather.3.cloned.1.call-update
  7.9 0.0 all-gather.5.cloned.1.call-start
  8.0 0.7 multiply_add_fusion.1
  8.7 60.8 %all-gather.3.cloned.1.call-done = bf16[4096,256]{1,0:T(8,128)(2,1)} async-done(((bf16[128,256]{1,0:T(8,128)(2,1)}), bf16[4096,256]{1,0:T(8,128)(2,1)}) %all-gather.3.cloned.1.call-update) | async-done | bytes 2097168 | tf_op jit(solution)/shard_map/all_gather | solution.py:36
  69.5 2.2 fusion.1
  71.8 0.3 fusion.19
  72.1 0.0 copy-done.10
  72.2 0.4 subtract_exponential_fusion.1
  72.6 0.5 fusion.16
  73.1 41.1 %all_gather.14 = bf16[1024,256]{1,0:T(8,128)(2,1)S(1)} all-gather(bf16[32,256]{1,0:T(8,128)(2,1)S(1)} %fusion.16), channel_id=1, replica_groups=mesh['tp'=32] {'tp'}, dimensions={0}, use_global_device_ids=true | all-gather | bytes 540672 | tf_op jit(solution)/shard_map/all_gather | solution.py:48
  114.2 0.5 fusion.17
  114.7 38.1 %all_gather.13 = bf16[1024,256]{1,0:T(8,128)(2,1)S(1)} all-gather(bf16[32,256]{1,0:T(8,128)(2,1)S(1)} %fusion.17), channel_id=1, replica_groups=mesh['tp'=32] {'tp'}, dimensions={0}, use_global_device_ids=true | all-gather | bytes 540672 | tf_op jit(solution)/shard_map/all_gather | solution.py:47
  152.8 1.5 fusion.23
  154.3 1.5 fusion.11
  155.8 7.6 %multiply_reduce_fusion = (f32[64,256]{1,0:T(8,128)S(1)}, f32[64,256,256]{2,1,0:T(8,128)}) fusion(f32[256,256]{1,0:T(8,128)S(1)} %dynamic-slice_convert_fusion.1, f32[256,256]{1,0:T(8,128)S(1)} %dynamic-slice_convert_fusion, f32[64,256]{1,0:T(8,128)S(1)} %fusion.11, f32[64,256,256]{2,1,0:T(8,128)S(1)} %copy-done.1, f32[256]{0:T(256)S(1)} %bitcast.56), kind=kLoop, calls=%fused_computation | loop fusion | flops 20955136 | bytes 34210816 | tf_op jit(solution)/shard_map/reduce_sum | solution.py:72
  163.4 1.1 fusion.12
  164.5 0.0 all-gather.5.cloned.1.call-update
  164.5 0.1 copy.19
  164.7 0.0 copy-done.2
  164.7 1.1 fusion.24
  165.8 49.9 %all-gather.5.cloned.1.call-done = bf16[2048,256]{1,0:T(8,128)(2,1)} async-done(((bf16[64,256]{1,0:T(8,128)(2,1)}), bf16[2048,256]{1,0:T(8,128)(2,1)}) %all-gather.5.cloned.1.call-update) | async-done | bytes 1048592 | tf_op jit(solution)/shard_map/all_gather | solution.py:76
  215.7 1.7 fusion.3
  217.4 0.7 copy.20
  (30 shorter events, 0.1 us)
Async XLA Ops:
  7.2 208.5 %copy-start = (bf16[128,2048]{1,0:T(8,128)(2,1)S(1)}, bf16[128,2048]{1,0:T(8,128)(2,1)}, u32[]{:S(2)}) copy-start(bf16[128,2048]{1,0:T(8,128)(2,1)} %param.26) | copy-start | bytes 1572868
  7.2 62.4 %all-gather.3.cloned.1.call-start = ((), (), s32[]{:S(2)}) async-start(), calls=%async_computation | async-start | bytes 2162688 | tf_op jit(solution)/shard_map/all_gather | solution.py:36
  7.2 65.4 %copy-start.4 = (bf16[32,4096]{1,0:T(8,128)(2,1)S(1)}, bf16[32,4096]{1,0:T(8,128)(2,1)}, u32[]{:S(2)}) copy-start(bf16[32,4096]{1,0:T(8,128)(2,1)} %param.19) | copy-start | bytes 786436
  7.2 106.9 %copy-start.5 = (bf16[32,4096]{1,0:T(8,128)(2,1)S(1)}, bf16[32,4096]{1,0:T(8,128)(2,1)}, u32[]{:S(2)}) copy-start(bf16[32,4096]{1,0:T(8,128)(2,1)} %param.18) | copy-start | bytes 786436
  7.9 207.7 %all-gather.5.cloned.1.call-start = ((), (), s32[]{:S(2)}) async-start(), calls=%async_computation.1 | async-start | bytes 1081344 | tf_op jit(solution)/shard_map/all_gather | solution.py:76
  8.7 63.1 %copy-start.7 = (bf16[4,4096]{1,0:T(4,128)(2,1)S(1)}, bf16[4,4096]{1,0:T(4,128)(2,1)}, u32[]{:S(2)}) copy-start(bf16[4,4096]{1,0:T(4,128)(2,1)} %param.22) | copy-start | bytes 98308
  8.7 63.1 %copy-start.11 = (f32[4]{0:T(128)S(1)}, f32[4]{0:T(128)}, u32[]{:S(2)}) copy-start(f32[4]{0:T(128)} %param.24) | copy-start | bytes 52
  8.7 63.4 %copy-start.8 = (bf16[4,4096]{1,0:T(4,128)(2,1)S(1)}, bf16[4,4096]{1,0:T(4,128)(2,1)}, u32[]{:S(2)}) copy-start(bf16[4,4096]{1,0:T(4,128)(2,1)} %param.23) | copy-start | bytes 98308
  8.7 63.5 %copy-start.10 = (f32[4,256]{1,0:T(4,128)S(1)}, f32[4,256]{1,0:T(4,128)}, u32[]{:S(2)}) copy-start(f32[4,256]{1,0:T(4,128)} %param.29) | copy-start | bytes 12292
  8.7 63.5 %copy-start.12 = (f32[4]{0:T(128)S(1)}, f32[4]{0:T(128)}, u32[]{:S(2)}) copy-start(f32[4]{0:T(128)} %param.25) | copy-start | bytes 52
  69.5 86.3 %copy-start.1 = (f32[64,256,256]{2,1,0:T(8,128)S(1)}, f32[64,256,256]{2,1,0:T(8,128)}, u32[]{:S(2)}) copy-start(f32[64,256,256]{2,1,0:T(8,128)} %param.27) | copy-start | bytes 50331652
  72.6 42.0 %copy-start.9 = (f32[4,256]{1,0:T(4,128)}, f32[4,256]{1,0:T(4,128)S(1)}, u32[]{:S(2)}) copy-start(f32[4,256]{1,0:T(4,128)S(1)} %get-tuple-element.11) | copy-start | bytes 12292
  155.8 7.6 %copy-start.3 = (bf16[64,4096]{1,0:T(8,128)(2,1)S(1)}, bf16[64,4096]{1,0:T(8,128)(2,1)}, u32[]{:S(2)}) copy-start(bf16[64,4096]{1,0:T(8,128)(2,1)} %param.21) | copy-start | bytes 1572868
  163.4 1.1 copy-start.6
  163.4 1.3 copy-start.2
Sparse Core Ops, SparseCore 0:
  10.8 58.6 all-gather.2
  164.6 50.9 all-gather.4
where the time goes:
time: 226 us; the launch traced here: 225 us
  waiting for transfers between devices  111 us (49%)
  blocking collectives  79.1 us (35%)
  between operations  14.3 us (6%)
  other arithmetic  13.1 us (6%)
  matrix products  5.98 us (3%)
    all_gather x1, waiting for transfers between devices, mix_block(): whole = lax.all_gather(rows, 'tp', axis=0, tiled=True).astype(jnp.float32)  60.8 us
    all_gather x1, waiting for transfers between devices, mix_block(): lax.all_gather(gated, 'tp', axis=0, tiled=True)  49.9 us
    all_gather x1, blocking collectives, mix_block(): lax.all_gather(key_loc, 'tp', axis=0, tiled=True)  41.1 us
    all_gather x1, blocking collectives, mix_block(): lax.all_gather(query_loc, 'tp', axis=0, tiled=True)  38.1 us
    reduce_sum x1, other arithmetic, mix_block(): numer = jnp.sum(q_head[None, :, :] * new_cells, axis=1)  7.56 us
  transfers between devices with their start and end apart: 2, of which 2 were waited for; matrix products, arithmetic and copies ran while one was open for 1% of the time, Pallas kernels for 0%

commit v1 on v0

--- a/solution.py
+++ b/solution.py
@@ -1,6 +1,10 @@
+import functools
+
 import jax
 import jax.numpy as jnp
 from jax import lax
+from jax.experimental import pallas as pl
+from jax.experimental.pallas import tpu as pltpu
 from jax.sharding import PartitionSpec as P
 
 DQK = 256
@@ -8,6 +12,450 @@
 
 
 EPS = 1e-06
+
+MESH = pl.DeviceIdType.MESH
+ANY = pl.BlockSpec(memory_space=pl.ANY)
+VM = pl.BlockSpec(memory_space=pltpu.VMEM)
+SIDES = (0, 2, 4, 6)
+
+
+def flip(me, mask):
+    out, bit = me, 1
+    while bit <= mask:
+        if mask & bit:
+            out = out + bit * (1 - 2 * ((me // bit) % 2))
+        bit *= 2
+    return out
+
+
+def greet(me, masks):
+    barrier = pltpu.get_barrier_semaphore()
+    for mask in masks:
+        pl.semaphore_signal(
+            barrier, inc=1, device_id=(flip(me, mask),), device_id_type=MESH
+        )
+    pl.semaphore_wait(barrier, len(masks))
+
+
+class Gather:
+    def __init__(self, me, planes, src, buf, send, recv):
+        self.me, self.planes, self.src, self.buf = me, planes, src, buf
+        self.send, self.recv = send, recv
+        self.rows = buf.shape[1]
+        self.sent, self.number = [], 0
+
+    def put(self, mask, origin_mask, slot, part=None):
+        origin = flip(self.me, origin_mask)
+        src = self.src if origin_mask == 0 else self.buf.at[origin]
+        dst = self.buf.at[origin]
+        if part is not None:
+            half = self.rows // 2
+            src = src.at[pl.ds(part * half, half)]
+            dst = dst.at[pl.ds(part * half, half)]
+        copy = pltpu.make_async_remote_copy(
+            src_ref=src,
+            dst_ref=dst,
+            send_sem=self.send.at[self.number],
+            recv_sem=self.recv.at[slot],
+            device_id=(flip(self.me, mask),),
+            device_id_type=MESH,
+        )
+        self.number += 1
+        copy.start()
+        self.sent.append(copy)
+
+    def got(self, origin_mask, slot, part=None):
+        dst = self.buf.at[flip(self.me, origin_mask)]
+        if part is not None:
+            half = self.rows // 2
+            dst = dst.at[pl.ds(part * half, half)]
+        pltpu.make_async_copy(dst, dst, self.recv.at[slot]).wait()
+
+    def begin(self):
+        for m in range(1, self.planes):
+            self.put(8 * m, 0, 10 * m)
+        self.put(2, 0, 1)
+        self.put(4, 0, 2)
+        self.put(1, 0, 5)
+
+    def z(self, m):
+        self.got(8 * m, 10 * m)
+        self.put(2, 8 * m, 10 * m + 1)
+        self.put(4, 8 * m, 10 * m + 2)
+        self.put(1, 8 * m, 10 * m + 5)
+
+    def x(self, m):
+        self.got(8 * m + 2, 10 * m + 1)
+        self.put(4, 8 * m + 2, 10 * m + 3, 0)
+        self.put(1, 8 * m + 2, 10 * m + 6)
+
+    def y(self, m):
+        self.got(8 * m + 4, 10 * m + 2)
+        self.put(2, 8 * m + 4, 10 * m + 4, 1)
+        self.put(1, 8 * m + 4, 10 * m + 7)
+
+    def d(self, m):
+        for part in range(2):
+            self.got(8 * m + 6, 10 * m + 3 + part, part)
+            self.put(1, 8 * m + 6, 10 * m + 8 + part, part)
+
+    def sibling(self, m, side):
+        origin = 8 * m + SIDES[side] + 1
+        if side == 3:
+            for part in range(2):
+                self.got(origin, 10 * m + 8 + part, part)
+        else:
+            self.got(origin, 10 * m + 5 + side)
+
+    def end(self):
+        for copy in self.sent:
+            copy.wait_send()
+
+    @staticmethod
+    def sends(planes):
+        return 10 * planes - 1
+
+    def events(self):
+        steps = []
+        for m in range(self.planes + 2):
+            if 1 <= m < self.planes:
+                steps.append((self.z, m, 0))
+            if 1 <= m <= self.planes:
+                steps.append((self.x, m - 1, 1))
+                steps.append((self.y, m - 1, 2))
+            if 2 <= m:
+                steps.append((self.d, m - 2, 3))
+        return steps
+
+
+def plane_masks(planes):
+    return [1, 2, 4] + [8 * m for m in range(1, planes)]
+
+
+def project_kernel(
+    planes, width, most,
+    tok, gain, w_q, w_k, w_v, w_o, w_i, w_f, b_i, b_f, where, maxima, cells,
+    c_out, val_out, og_out, q_out, k_out, kown_out, max_out, dec_out, fre_out,
+    buf, wbuf, gcol, acc, total, qk_own, qk_all,
+    send, recv, qsend, qrecv, wsem, csem,
+):
+    me = lax.axis_index("tp")
+    loads = []
+    row = 0
+    for number, ref in enumerate((w_q, w_k, w_v, w_o)):
+        copy = pltpu.make_async_copy(
+            ref, wbuf.at[pl.ds(row, ref.shape[0])], wsem.at[number]
+        )
+        copy.start()
+        loads.append(copy)
+        row += ref.shape[0]
+    big = pltpu.make_async_copy(cells, c_out, csem)
+    masks = plane_masks(planes) + [6]
+    greet(me, masks)
+    g = Gather(me, planes, tok, buf, send, recv)
+    g.begin()
+    big.start()
+    buf[me] = tok[...]
+    heads = w_i.shape[0]
+    gates = jnp.concatenate(
+        [w_i[...].astype(jnp.float32), w_f[...].astype(jnp.float32)], axis=0
+    )
+    wbuf[row : row + 16] = jnp.concatenate([gates, gates], axis=0).astype(jnp.bfloat16)
+    rows = tok.shape[0]
+    for part in range(width // 128):
+        line = gain[part : part + 1, :]
+        gcol[part * 128 : (part + 1) * 128] = jnp.transpose(
+            jnp.broadcast_to(line, (128, 128))
+        )
+    acc[...] = jnp.zeros_like(acc)
+    total[...] = jnp.zeros_like(total)
+    for copy in loads:
+        copy.wait()
+
+    def take(m, side):
+        g.sibling(m, side)
+        chip = flip(me, 8 * m + SIDES[side]) // 2
+        block = buf[pl.ds(chip * 2, 2)].astype(jnp.float32)
+        block = block.reshape(2 * rows, block.shape[2])
+        at = pl.multiple_of(chip * 2 * rows, 2 * rows)
+        gains = gcol[pl.ds(at, 2 * rows), :]
+        gains = jnp.concatenate([gains] * (block.shape[1] // 128), axis=1)
+        normed = (block * gains).astype(jnp.bfloat16)
+        squares = block * block
+        total[...] += jnp.sum(squares.reshape(-1, 8, squares.shape[1]), axis=0)
+        acc[...] += jnp.dot(
+            wbuf[:, pl.ds(at, 2 * rows)], normed, preferred_element_type=jnp.float32
+        )
+
+    ready = [(0, 0)]
+    for step, m, side in g.events():
+        step(m)
+        if ready:
+            take(*ready.pop(0))
+        ready.append((m, side))
+    for item in ready:
+        take(*item)
+
+    scale = lax.rsqrt(jnp.sum(total[...], axis=0, keepdims=True) / width + EPS)
+    nq = w_q.shape[0]
+    nv = w_v.shape[0]
+    q = (acc[0:nq] * scale).astype(jnp.bfloat16)
+    k = (acc[nq : 2 * nq] * scale * DQK ** (-0.5)).astype(jnp.bfloat16)
+    qk_own[0:nq] = q
+    qk_own[nq : 2 * nq] = k
+    mine = lax.rem(me, 8)
+    copies = []
+
+    def pass_on(mask, src, origin, slot):
+        copy = pltpu.make_async_remote_copy(
+            src_ref=src,
+            dst_ref=qk_all.at[origin],
+            send_sem=qsend.at[len(copies)],
+            recv_sem=qrecv.at[slot],
+            device_id=(flip(me, mask),),
+            device_id_type=MESH,
+        )
+        copy.start()
+        copies.append(copy)
+
+    def arrived(origin, slot):
+        ref = qk_all.at[origin]
+        pltpu.make_async_copy(ref, ref, qrecv.at[slot]).wait()
+
+    for mask in (6, 2, 4, 1):
+        pass_on(mask, qk_own, mine, mask)
+    qk_all[mine] = qk_own[...]
+    kown_out[...] = k
+    gate_in = acc[row : row + heads] * scale + b_i[...]
+    gate_f = acc[row + heads : row + 2 * heads] * scale + b_f[...]
+    soft = jnp.minimum(gate_f, 0.0) - jnp.log1p(jnp.exp(-jnp.abs(gate_f)))
+    logf = soft * (1.0 + where[...].astype(jnp.float32) / most)
+    lifted = logf + maxima[...]
+    new_max = jnp.maximum(lifted, gate_in)
+    max_out[...] = new_max
+    dec_out[...] = jnp.exp(lifted - new_max)
+    fre_out[...] = jnp.exp(gate_in - new_max)
+    val_out[...] = acc[2 * nq : 2 * nq + nv] * scale
+    og_out[...] = jax.nn.sigmoid(acc[2 * nq + nv : 2 * nq + 2 * nv] * scale)
+    for mask in (2, 4, 6):
+        origin = flip(mine, mask)
+        arrived(origin, mask)
+        pass_on(1, qk_all.at[origin], origin, mask + 1)
+    for mask in (1, 3, 5, 7):
+        arrived(flip(mine, mask), mask)
+    for part in range(8):
+        q_out[part * nq : (part + 1) * nq] = qk_all[part, 0:nq].astype(jnp.float32)
+        k_out[part * nq : (part + 1) * nq] = qk_all[part, nq : 2 * nq].astype(jnp.float32)
+    for copy in copies:
+        copy.wait_send()
+    g.end()
+    big.wait()
+
+
+GROUP = 4
+SLOTS = 4
+
+
+def cell_kernel(
+    cells, val, og, q, k, dec, fre, norms,
+    new_cells, gated,
+    stage, numer, fv, nrm, den, sems, nsem,
+):
+    me = lax.axis_index("tp")
+    head = me * dec.shape[0] // lax.axis_size("tp")
+    dq = q.shape[0]
+    load = pltpu.make_async_copy(norms.at[pl.ds(head * dq, dq)], nrm, nsem)
+    load.start()
+    decay = dec[pl.ds(head, 1), :]
+    fresh = fre[pl.ds(head, 1), :]
+    fv[...] = fresh * val[...]
+    seqs = decay.shape[1]
+    decay8 = jnp.broadcast_to(decay, (8, seqs))
+    number = cells.shape[0] // GROUP
+
+    def out_copy(step, slot):
+        return pltpu.make_async_copy(
+            stage.at[slot], new_cells.at[pl.ds(step * GROUP, GROUP)], sems.at[slot]
+        )
+
+    def body(step, carry):
+        slot = lax.rem(step, SLOTS)
+
+        @pl.when(step >= SLOTS)
+        def _():
+            out_copy(step - SLOTS, slot).wait()
+
+        lines = [
+            jnp.broadcast_to(fv[pl.ds(step * GROUP + i, 1), :], (8, seqs))
+            for i in range(GROUP)
+        ]
+        sums = [jnp.zeros((8, seqs), jnp.float32)] * GROUP
+        for d in range(0, dq, 8):
+            qd, kd = q[d : d + 8], k[d : d + 8]
+            for i in range(GROUP):
+                new = decay8 * cells[step * GROUP + i, d : d + 8] + lines[i] * kd
+                stage[slot, i, d : d + 8] = new
+                sums[i] = sums[i] + qd * new
+        for i in range(GROUP):
+            numer[pl.ds(step * GROUP + i, 1), :] = jnp.sum(
+                sums[i], axis=0, keepdims=True
+            )
+        out_copy(step, slot).start()
+        return carry
+
+    lax.fori_loop(0, number, body, 0)
+    load.wait()
+    denom = jnp.sum(q[...] * (decay * nrm[...] + fresh * k[...]), axis=0, keepdims=True)
+    hidden = numer[...] / jnp.maximum(jnp.abs(denom), 1.0)
+    gated[...] = (hidden * og[...]).astype(jnp.bfloat16)
+    for step in range(number - SLOTS, number):
+        out_copy(step, step % SLOTS).wait()
+
+
+def read_kernel(
+    planes, gated, kown, w_read, tok, mixed, keys, gbuf, wbuf,
+    send, recv, ksend, krecv, wsem,
+):
+    me = lax.axis_index("tp")
+    load = pltpu.make_async_copy(w_read, wbuf, wsem)
+    load.start()
+    greet(me, plane_masks(planes))
+    g = Gather(me, planes, gated, gbuf, send, recv)
+    h = Gather(me, planes, kown, keys, ksend, krecv)
+    g.begin()
+    h.begin()
+    gbuf[me] = gated[...]
+    keys[me] = kown[...]
+    for (step, m, _), (other, _, _) in zip(g.events(), h.events()):
+        step(m)
+        other(m)
+    for m in range(planes):
+        for side in range(4):
+            g.sibling(m, side)
+    load.wait()
+    whole = gbuf[...].reshape(-1, gbuf.shape[2])
+    out = jnp.dot(wbuf[...], whole, preferred_element_type=jnp.float32)
+    mixed[...] = (tok[...].astype(jnp.float32) + out).astype(jnp.bfloat16)
+    for m in range(planes):
+        for side in range(4):
+            h.sibling(m, side)
+    g.end()
+    h.end()
+
+
+def fused_block(
+    rows, where, gain, w_query, w_key, w_value, w_outgate, w_input, w_forget,
+    bias_input, bias_forget, w_read, cells, norms, maxima,
+):
+    count = lax.axis_size("tp")
+    planes = count // 8
+    width = gain.shape[0]
+    heads = w_input.shape[0]
+    seqs = rows.shape[1]
+    nq, nv = w_query.shape[0], w_value.shape[0]
+    f32, bf16 = jnp.float32, jnp.bfloat16
+    total_w = 2 * nq + 2 * nv + 16
+    sends = Gather.sends(planes)
+    dma = pltpu.SemaphoreType.DMA
+    c_vm, val, og, q, k, kown, new_max, dec, fre = pl.pallas_call(
+        functools.partial(project_kernel, planes, width, MOST_LEN),
+        out_shape=(
+            pltpu.VMEM(cells.shape, f32),
+            jax.ShapeDtypeStruct((nv, seqs), f32),
+            jax.ShapeDtypeStruct((nv, seqs), f32),
+            jax.ShapeDtypeStruct((8 * nq, seqs), f32),
+            jax.ShapeDtypeStruct((8 * nq, seqs), f32),
+            jax.ShapeDtypeStruct((nq, seqs), bf16),
+            jax.ShapeDtypeStruct((heads, seqs), f32),
+            jax.ShapeDtypeStruct((heads, seqs), f32),
+            jax.ShapeDtypeStruct((heads, seqs), f32),
+        ),
+        in_specs=[VM, VM, ANY, ANY, ANY, ANY] + [VM] * 6 + [ANY],
+        out_specs=[VM] * 9,
+        scratch_shapes=[
+            pltpu.VMEM((count, rows.shape[0], seqs), bf16),
+            pltpu.VMEM((total_w, width), bf16),
+            pltpu.VMEM((width, 128), f32),
+            pltpu.VMEM((total_w, seqs), f32),
+            pltpu.VMEM((8, seqs), f32),
+            pltpu.VMEM((2 * nq, seqs), bf16),
+            pltpu.VMEM((8, 2 * nq, seqs), bf16),
+            dma((sends,)),
+            dma((10 * planes,)),
+            dma((7,)),
+            dma((8,)),
+            dma((4,)),
+            dma,
+        ],
+        compiler_params=pltpu.CompilerParams(
+            collective_id=0, has_side_effects=True, vmem_limit_bytes=K1_LIMIT
+        ),
+        name="project",
+    )(
+        rows, gain.reshape(width // 128, 128), w_query, w_key, w_value, w_outgate,
+        w_input, w_forget, bias_input[:, None], bias_forget[:, None],
+        where[None, :], maxima, cells,
+    )
+    new_cells, gated = pl.pallas_call(
+        cell_kernel,
+        out_shape=(
+            jax.ShapeDtypeStruct(cells.shape, f32),
+            jax.ShapeDtypeStruct((nv, seqs), bf16),
+        ),
+        in_specs=[VM] * 7 + [ANY],
+        out_specs=[ANY, VM],
+        scratch_shapes=[
+            pltpu.VMEM((SLOTS, GROUP) + cells.shape[1:], f32),
+            pltpu.VMEM((nv, seqs), f32),
+            pltpu.VMEM((nv, seqs), f32),
+            pltpu.VMEM((8 * nq, seqs), f32),
+            pltpu.VMEM((8, seqs), f32),
+            dma((SLOTS,)),
+            dma,
+        ],
+        compiler_params=pltpu.CompilerParams(vmem_limit_bytes=K1_LIMIT),
+        name="cells",
+    )(c_vm, val, og, q, k, dec, fre, norms)
+    mixed, keys = pl.pallas_call(
+        functools.partial(read_kernel, planes),
+        out_shape=(
+            jax.ShapeDtypeStruct(rows.shape, bf16),
+            jax.ShapeDtypeStruct((count, nq, seqs), bf16),
+        ),
+        in_specs=[VM, VM, ANY, VM],
+        out_specs=[VM, VM],
+        scratch_shapes=[
+            pltpu.VMEM((count, nv, seqs), bf16),
+            pltpu.VMEM(w_read.shape, bf16),
+            dma((sends,)),
+            dma((10 * planes,)),
+            dma((sends,)),
+            dma((10 * planes,)),
+            dma,
+        ],
+        compiler_params=pltpu.CompilerParams(
+            collective_id=1, has_side_effects=True, vmem_limit_bytes=K1_LIMIT
+        ),
+        name="readout",
+    )(gated, kown, w_read, rows)
+    keys = keys.astype(f32).reshape(heads, -1, seqs)
+    norms_new = dec[:, None, :] * norms.reshape(keys.shape) + fre[:, None, :] * keys
+    return mixed, new_cells, norms_new.reshape(norms.shape), new_max
+
+
+K1_LIMIT = 30 * 1024 * 1024
+
+
+def fits(count, rows, w_query, w_input, cells):
+    planes = count // 8
+    return (
+        count % 8 == 0
+        and planes & (planes - 1) == 0
+        and w_input.shape[0] == planes
+        and rows.shape[0] % 128 == 0
+        and w_query.shape[0] % 32 == 0
+        and cells.shape[0] % (GROUP * SLOTS) == 0
+    )
 
 
 def mix_block(
@@ -96,9 +544,11 @@
     norms,
     maxima,
 ):
-    row_parts, cell_parts, norm_parts, max_parts = ([], [], [], [])
-    where = positions.astype(jnp.float32)[None, :]
-    rows, cell_new, norm_new, max_new = mix_block(
+    if fits(lax.axis_size("tp"), tokens, w_query, w_input, cells):
+        block, where = fused_block, positions
+    else:
+        block, where = mix_block, positions.astype(jnp.float32)[None, :]
+    return block(
         tokens,
         where,
         norm_gain,
@@ -115,11 +565,6 @@
         norms,
         maxima,
     )
-    row_parts.append(rows)
-    cell_parts.append(cell_new)
-    norm_parts.append(norm_new)
-    max_parts.append(max_new)
-    return (row_parts[0], cell_parts[0], norm_parts[0], max_parts[0])
 
 
 def solution(mesh):

time: 226 us -> 76.4 us (0.34)
  waiting for transfers between devices: 111 us -> 0 us
  blocking collectives: 79.1 us -> 0 us
  Pallas kernels: 0 us -> 50.8 us
  local copies, waits for them, and re-layouts: 0.98 us -> 23.1 us
  between operations: 14.3 us -> 0.7 us
  other arithmetic: 13.1 us -> 1.15 us
  matrix products: 5.98 us -> 0 us
    all_gather x2 -> x0, waiting for transfers between devices: 111 us -> none  [the longest x1 60.8 us: mix_block(): whole = lax.all_gather(rows, 'tp', axis=0, tiled=True).astype(jnp.float32)]
    all_gather x2 -> x0, blocking collectives: 79.1 us -> none  [the longest x1 41.1 us: mix_block(): lax.all_gather(key_loc, 'tp', axis=0, tiled=True)]
    pallas_call x0 -> x3, Pallas kernels: none -> 50.8 us  [the longest x1 26.2 us: fused_block(): pl.pallas_call(functools.partial(project_kernel, planes, width, MOST_LEN)...]
    unnamed x28 -> x32, local copies, waits for them, and re-layouts: 0.97 us -> 21.6 us
    reduce_sum x3 -> x0, other arithmetic: 11.2 us -> none  [the longest x1 7.56 us: mix_block(): numer = jnp.sum(q_head[None, :, :] * new_cells, axis=1)]
    dot_general x7 -> x0, matrix products: 5.98 us -> none  [the longest x1 1.7 us: mix_block(): jnp.dot(w_read, lax.all_gather(gated, 'tp', axis=0, tiled=True), preferre...]
  transfers between devices with their start and end apart: 2 -> 0, of which waited for: 2 -> 0; matrix products, arithmetic and copies ran while one was open for 1% -> 0% of each run, Pallas kernels for 0% -> 0%
where the time goes in v1:
time: 76.4 us; the launch traced here: 75.7 us
  Pallas kernels  50.8 us (66%)
  local copies, waits for them, and re-layouts  23.1 us (30%)
  other arithmetic  1.15 us (2%)
    pallas_call x1, Pallas kernels, fused_block(): pl.pallas_call(functools.partial(project_kernel, planes, width, MOST_LEN)...  26.2 us
    unnamed x32, local copies, waits for them, and re-layouts  21.6 us
    pallas_call x1, Pallas kernels, fused_block(): pl.pallas_call(functools.partial(read_kernel, planes), out_shape=(jax.Sha...  18.5 us
    pallas_call x1, Pallas kernels, fused_block(): pl.pallas_call(cell_kernel, out_shape=(jax.ShapeDtypeStruct(cells.shape,...  6.07 us

profile of v1, /device:TPU:1, one launch (start us, length us, event | category | flops | bytes accessed | tf_op | source)
XLA Modules:
  0.0 75.7 jit_solution(17308761458748980620)
XLA Ops:
  0.6 0.0 copy-start.2
  0.6 0.8 %copy.19.b_i = f32[4,1]{1,0:T(4,128)S(1)} copy(f32[4,1]{0,1:T(1,128)} %bitcast.15) | data formatting | bytes 32 | tf_op jit(solution)/shard_map/broadcast_in_dim | solution.py:396
  1.5 0.7 copy.20.b_f
  2.2 1.0 %copy-done.3 = bf16[64,4096]{1,0:T(8,128)(2,1)S(1)} copy-done((bf16[64,4096]{1,0:T(8,128)(2,1)S(1)}, bf16[64,4096]{1,0:T(8,128)(2,1)}, u32[]{:S(2)}) %copy-start.3) | copy-done | bytes 524312
  3.3 1.0 %copy-done.4 = bf16[64,4096]{1,0:T(8,128)(2,1)S(1)} copy-done((bf16[64,4096]{1,0:T(8,128)(2,1)S(1)}, bf16[64,4096]{1,0:T(8,128)(2,1)}, u32[]{:S(2)}) %copy-start.4) | copy-done | bytes 524312
  4.3 0.9 %copy-done.6 = bf16[32,4096]{1,0:T(8,128)(2,1)S(1)} copy-done((bf16[32,4096]{1,0:T(8,128)(2,1)S(1)}, bf16[32,4096]{1,0:T(8,128)(2,1)}, u32[]{:S(2)}) %copy-start.6) | copy-done | bytes 262168
  5.2 0.9 %copy-done.7 = bf16[32,4096]{1,0:T(8,128)(2,1)S(1)} copy-done((bf16[32,4096]{1,0:T(8,128)(2,1)S(1)}, bf16[32,4096]{1,0:T(8,128)(2,1)}, u32[]{:S(2)}) %copy-start.7) | copy-done | bytes 262168
  6.2 0.8 %copy-done.8 = bf16[128,256]{1,0:T(8,128)(2,1)S(1)} copy-done((bf16[128,256]{1,0:T(8,128)(2,1)S(1)}, bf16[128,256]{1,0:T(8,128)(2,1)}, u32[]{:S(2)}) %copy-start.8) | copy-done | bytes 65560
  7.0 0.8 copy-done.10
  7.8 0.8 copy-done.11
  8.6 0.7 copy-done.12
  9.3 0.7 copy-done.13
  10.0 0.7 copy-done.14
  10.6 26.2 %project.1 = (f32[64,256,256]{2,1,0:T(8,128)S(1)}, f32[64,256]{1,0:T(8,128)S(1)}, f32[64,256]{1,0:T(8,128)S(1)}, f32[256,256]{1,0:T(8,128)S(1)}, f32[256,256]{1,...) custom-call(bf16[128,256]{1,0:T(8,128)(2,1)S(1)} %copy-done.8, ...), custom_call_target="tpu_custom_call" | custom-call | tf_op jit(solution)/shard_map/project/pallas_call | solution.py:360
  36.8 0.0 copy-start
  36.8 6.2 %copy-done = f32[64,256,256]{2,1,0:T(8,128)} copy-done((f32[64,256,256]{2,1,0:T(8,128)}, f32[64,256,256]{2,1,0:T(8,128)S(1)}, u32[]{:S(2)}) %copy-start) | copy-done | bytes 16777240
  43.0 5.8 %copy-done.1 = f32[64,256,256]{2,1,0:T(8,128)S(1)} copy-done((f32[64,256,256]{2,1,0:T(8,128)S(1)}, f32[64,256,256]{2,1,0:T(8,128)}, u32[]{:S(2)}) %copy-start.1) | copy-done | bytes 16777240
  48.7 6.1 %cells.3 = (f32[64,256,256]{2,1,0:T(8,128)}, bf16[64,256]{1,0:T(8,128)(2,1)S(1)}) custom-call(f32[64,256,256]{2,1,0:T(8,128)S(1)} %copy-done.1, f32[64,256]{1,0:T(8,128)S(1)} %get-tuple-element.18.val, f32[64,256]{1,0:T(8,128)S(1)} %get-tuple-element.19.og, f32[256,256]{1,0:T(8,128)S(1)} %get-tuple-element.20.q, f32[256,256]{1,0:T(8,128)S(1)} %get-tuple-element.21.k, ...), custom_call_target="tpu_custom_call" | custom-call | tf_op jit(solution)/shard_map/cells/pallas_call | solution.py:399
  54.8 0.0 copy-done.5
  54.8 0.0 copy-done.9
  54.8 18.5 %readout.1 = (bf16[128,256]{1,0:T(8,128)(2,1)S(1)}, bf16[32,32,256]{2,1,0:T(8,128)(2,1)S(1)}) custom-call(bf16[64,256]{1,0:T(8,128)(2,1)S(1)} %get-tuple-element.24.gated, bf16[32,256]{1,0:T(8,128)(2,1)S(1)} %get-tuple-element.25.kown, bf16[128,2048]{1,0:T(8,128)(2,1)S(1)} %copy-done.5, bf16[128,256]{1,0:T(8,128)(2,1)S(1)} %copy-done.9), custom_call_target="tpu_custom_call" | custom-call | tf_op jit(solution)/shard_map/readout/pallas_call | solution.py:419
  73.4 1.1 %fusion = f32[1024,256]{1,0:T(8,128)} fusion(f32[1024,256]{1,0:T(8,128)S(1)} %copy-done.2, bf16[32,32,256]{2,1,0:T(8,128)(2,1)S(1)} %get-tuple-element.28, f32[4,256]{1,0:T(4,128)S(1)} %get-tuple-element.23.fre, f32[4,256]{1,0:T(4,128)S(1)} %get-tuple-element.22.dec), kind=kLoop, calls=%fused_computation.1 | loop fusion | flops 1048576 | bytes 2629632 | tf_op jit(solution)/shard_map/add | solution.py:442
  74.5 0.6 copy.23
  75.2 0.6 copy.24
  (14 shorter events, 0.0 us)
Async XLA Ops:
  0.6 42.3 %copy-start.2 = (f32[1024,256]{1,0:T(8,128)S(1)}, f32[1024,256]{1,0:T(8,128)}, u32[]{:S(2)}) copy-start(f32[1024,256]{1,0:T(8,128)} %norms.1) | copy-start | bytes 3145732
  2.2 1.0 %copy-start.3 = (bf16[64,4096]{1,0:T(8,128)(2,1)S(1)}, bf16[64,4096]{1,0:T(8,128)(2,1)}, u32[]{:S(2)}) copy-start(bf16[64,4096]{1,0:T(8,128)(2,1)} %w_v.1) | copy-start | bytes 1572868
  3.3 1.0 %copy-start.4 = (bf16[64,4096]{1,0:T(8,128)(2,1)S(1)}, bf16[64,4096]{1,0:T(8,128)(2,1)}, u32[]{:S(2)}) copy-start(bf16[64,4096]{1,0:T(8,128)(2,1)} %w_o.1) | copy-start | bytes 1572868
  4.3 0.9 %copy-start.6 = (bf16[32,4096]{1,0:T(8,128)(2,1)S(1)}, bf16[32,4096]{1,0:T(8,128)(2,1)}, u32[]{:S(2)}) copy-start(bf16[32,4096]{1,0:T(8,128)(2,1)} %w_q.1) | copy-start | bytes 786436
  5.2 0.9 %copy-start.7 = (bf16[32,4096]{1,0:T(8,128)(2,1)S(1)}, bf16[32,4096]{1,0:T(8,128)(2,1)}, u32[]{:S(2)}) copy-start(bf16[32,4096]{1,0:T(8,128)(2,1)} %w_k.1) | copy-start | bytes 786436
  6.2 0.8 %copy-start.8 = (bf16[128,256]{1,0:T(8,128)(2,1)S(1)}, bf16[128,256]{1,0:T(8,128)(2,1)}, u32[]{:S(2)}) copy-start(bf16[128,256]{1,0:T(8,128)(2,1)} %tok.3) | copy-start | bytes 196612
  7.0 0.8 %copy-start.10 = (bf16[4,4096]{1,0:T(4,128)(2,1)S(1)}, bf16[4,4096]{1,0:T(4,128)(2,1)}, u32[]{:S(2)}) copy-start(bf16[4,4096]{1,0:T(4,128)(2,1)} %w_i.1) | copy-start | bytes 98308
  7.8 0.8 %copy-start.11 = (bf16[4,4096]{1,0:T(4,128)(2,1)S(1)}, bf16[4,4096]{1,0:T(4,128)(2,1)}, u32[]{:S(2)}) copy-start(bf16[4,4096]{1,0:T(4,128)(2,1)} %w_f.1) | copy-start | bytes 98308
  8.6 0.7 copy-start.12
  9.3 0.7 copy-start.13
  10.0 0.7 copy-start.14
  10.6 44.2 %copy-start.5 = (bf16[128,2048]{1,0:T(8,128)(2,1)S(1)}, bf16[128,2048]{1,0:T(8,128)(2,1)}, u32[]{:S(2)}) copy-start(bf16[128,2048]{1,0:T(8,128)(2,1)} %w_read.1) | copy-start | bytes 1572868
  10.6 44.2 %copy-start.9 = (bf16[128,256]{1,0:T(8,128)(2,1)S(1)}, bf16[128,256]{1,0:T(8,128)(2,1)}, u32[]{:S(2)}) copy-start(bf16[128,256]{1,0:T(8,128)(2,1)} %tok.3) | copy-start | bytes 196612
  36.8 6.2 %copy-start = (f32[64,256,256]{2,1,0:T(8,128)}, f32[64,256,256]{2,1,0:T(8,128)S(1)}, u32[]{:S(2)}) copy-start(f32[64,256,256]{2,1,0:T(8,128)S(1)} %get-tuple-element.17.cells) | copy-start | bytes 50331652
  43.0 5.8 %copy-start.1 = (f32[64,256,256]{2,1,0:T(8,128)S(1)}, f32[64,256,256]{2,1,0:T(8,128)}, u32[]{:S(2)}) copy-start(f32[64,256,256]{2,1,0:T(8,128)} %copy-done) | copy-start | bytes 50331652

commit v2 on v1

--- a/solution.py
+++ b/solution.py
@@ -14,7 +14,7 @@
 EPS = 1e-06
 
 MESH = pl.DeviceIdType.MESH
-ANY = pl.BlockSpec(memory_space=pl.ANY)
+ANY = pl.BlockSpec(memory_space=pltpu.HBM)
 VM = pl.BlockSpec(memory_space=pltpu.VMEM)
 SIDES = (0, 2, 4, 6)
 
@@ -134,12 +134,24 @@
 
 def project_kernel(
     planes, width, most,
-    tok, gain, w_q, w_k, w_v, w_o, w_i, w_f, b_i, b_f, where, maxima, cells,
+    tok_in, gain_in, w_q, w_k, w_v, w_o, wi_in, wf_in, bi_in, bf_in, where_in,
+    maxima_in, cells,
     c_out, val_out, og_out, q_out, k_out, kown_out, max_out, dec_out, fre_out,
     buf, wbuf, gcol, acc, total, qk_own, qk_all,
-    send, recv, qsend, qrecv, wsem, csem,
+    tok, gain, w_i, w_f, b_i, b_f, where, maxima,
+    send, recv, qsend, qrecv, wsem, csem, ssem,
 ):
     me = lax.axis_index("tp")
+    small = []
+    for number, (ref, here) in enumerate(
+        (
+            (tok_in, tok), (wi_in, w_i), (wf_in, w_f), (gain_in, gain),
+            (bi_in, b_i), (bf_in, b_f), (where_in, where), (maxima_in, maxima),
+        )
+    ):
+        copy = pltpu.make_async_copy(ref, here, ssem.at[number])
+        copy.start()
+        small.append(copy)
     loads = []
     row = 0
     for number, ref in enumerate((w_q, w_k, w_v, w_o)):
@@ -153,8 +165,11 @@
     masks = plane_masks(planes) + [6]
     greet(me, masks)
     g = Gather(me, planes, tok, buf, send, recv)
+    small[0].wait()
     g.begin()
     big.start()
+    for copy in small[1:]:
+        copy.wait()
     buf[me] = tok[...]
     heads = w_i.shape[0]
     gates = jnp.concatenate(
@@ -226,8 +241,14 @@
         pass_on(mask, qk_own, mine, mask)
     qk_all[mine] = qk_own[...]
     kown_out[...] = k
-    gate_in = acc[row : row + heads] * scale + b_i[...]
-    gate_f = acc[row + heads : row + 2 * heads] * scale + b_f[...]
+    def column(line):
+        return jnp.concatenate(
+            [jnp.broadcast_to(line[:, i : i + 1], scale.shape) for i in range(heads)],
+            axis=0,
+        )
+
+    gate_in = acc[row : row + heads] * scale + column(b_i)
+    gate_f = acc[row + heads : row + 2 * heads] * scale + column(b_f)
     soft = jnp.minimum(gate_f, 0.0) - jnp.log1p(jnp.exp(-jnp.abs(gate_f)))
     logf = soft * (1.0 + where[...].astype(jnp.float32) / most)
     lifted = logf + maxima[...]
@@ -356,6 +377,9 @@
     f32, bf16 = jnp.float32, jnp.bfloat16
     total_w = 2 * nq + 2 * nv + 16
     sends = Gather.sends(planes)
+    hbm = functools.partial(
+        pltpu.with_memory_space_constraint, memory_space=pltpu.HBM
+    )
     dma = pltpu.SemaphoreType.DMA
     c_vm, val, og, q, k, kown, new_max, dec, fre = pl.pallas_call(
         functools.partial(project_kernel, planes, width, MOST_LEN),
@@ -370,7 +394,7 @@
             jax.ShapeDtypeStruct((heads, seqs), f32),
             jax.ShapeDtypeStruct((heads, seqs), f32),
         ),
-        in_specs=[VM, VM, ANY, ANY, ANY, ANY] + [VM] * 6 + [ANY],
+        in_specs=[ANY] * 13,
         out_specs=[VM] * 9,
         scratch_shapes=[
             pltpu.VMEM((count, rows.shape[0], seqs), bf16),
@@ -380,21 +404,35 @@
             pltpu.VMEM((8, seqs), f32),
             pltpu.VMEM((2 * nq, seqs), bf16),
             pltpu.VMEM((8, 2 * nq, seqs), bf16),
+            pltpu.VMEM(rows.shape, bf16),
+            pltpu.VMEM((width // 128, 128), f32),
+            pltpu.VMEM(w_input.shape, bf16),
+            pltpu.VMEM(w_forget.shape, bf16),
+            pltpu.VMEM((1, heads), f32),
+            pltpu.VMEM((1, heads), f32),
+            pltpu.VMEM((1, seqs), where.dtype),
+            pltpu.VMEM((heads, seqs), f32),
             dma((sends,)),
             dma((10 * planes,)),
             dma((7,)),
             dma((8,)),
             dma((4,)),
             dma,
+            dma((8,)),
         ],
         compiler_params=pltpu.CompilerParams(
             collective_id=0, has_side_effects=True, vmem_limit_bytes=K1_LIMIT
         ),
         name="project",
     )(
-        rows, gain.reshape(width // 128, 128), w_query, w_key, w_value, w_outgate,
-        w_input, w_forget, bias_input[:, None], bias_forget[:, None],
-        where[None, :], maxima, cells,
+        *map(
+            hbm,
+            (
+                rows, gain.reshape(width // 128, 128), w_query, w_key, w_value,
+                w_outgate, w_input, w_forget, bias_input[None, :],
+                bias_forget[None, :], where[None, :], maxima, cells,
+            ),
+        )
     )
     new_cells, gated = pl.pallas_call(
         cell_kernel,
@@ -415,7 +453,9 @@
         ],
         compiler_params=pltpu.CompilerParams(vmem_limit_bytes=K1_LIMIT),
         name="cells",
-    )(c_vm, val, og, q, k, dec, fre, norms)
+    )(
+        pltpu.with_memory_space_constraint(c_vm, memory_space=pltpu.VMEM), val, og, q, k, dec, fre, norms,
+    )
     mixed, keys = pl.pallas_call(
         functools.partial(read_kernel, planes),
         out_shape=(

time: 76.4 us -> 54.1 us (0.71)
  local copies, waits for them, and re-layouts: 23.1 us -> 1.23 us
    unnamed x32 -> x8, local copies, waits for them, and re-layouts: 21.6 us -> 1.23 us
    broadcast_in_dim x2 -> x0, local copies, waits for them, and re-layouts: 1.57 us -> none  [the longest x1 0.83 us: fused_block(): bias_input[:, None]]
where the time goes in v2:
time: 54.1 us; the launch traced here: 53.9 us
  Pallas kernels  50.8 us (94%)
  local copies, waits for them, and re-layouts  1.23 us (2%)
  other arithmetic  1.19 us (2%)
  between operations  0.71 us (1%)
    pallas_call x1, Pallas kernels, fused_block(): pl.pallas_call(functools.partial(project_kernel, planes, width, MOST_LEN)...  26.3 us
    pallas_call x1, Pallas kernels, fused_block(): pl.pallas_call(functools.partial(read_kernel, planes), out_shape=(jax.Sha...  18.4 us
    pallas_call x1, Pallas kernels, fused_block(): pl.pallas_call(cell_kernel, out_shape=(jax.ShapeDtypeStruct(cells.shape,...  6.09 us
    unnamed x8, local copies, waits for them, and re-layouts  1.23 us
    add x1, other arithmetic, fused_block(): dec[:, None, :] * norms.reshape(keys.shape) + fre[:, None, :] * keys  1.19 us

profile of v2, /device:TPU:1, one launch (start us, length us, event | category | flops | bytes accessed | tf_op | source)
XLA Modules:
  0.0 53.9 jit_solution(17454840956633485559)
XLA Ops:
  0.6 0.0 copy-start
  0.6 0.0 copy-start.1
  0.7 0.0 copy-start.2
  0.7 26.3 %project.1 = (f32[64,256,256]{2,1,0:T(8,128)S(1)}, f32[64,256]{1,0:T(8,128)S(1)}, f32[64,256]{1,0:T(8,128)S(1)}, f32[256,256]{1,0:T(8,128)S(1)}, f32[256,256]{1,...) custom-call(bf16[128,256]{1,0:T(8,128)(2,1)} %tok.1, ...), custom_call_target="tpu_custom_call" | custom-call | tf_op jit(solution)/shard_map/project/pallas_call | solution.py:384
  27.0 0.0 copy-done
  27.0 6.1 %cells.3 = (f32[64,256,256]{2,1,0:T(8,128)}, bf16[64,256]{1,0:T(8,128)(2,1)S(1)}) custom-call(f32[64,256,256]{2,1,0:T(8,128)S(1)} %get-tuple-element.17.cells, f32[64,256]{1,0:T(8,128)S(1)} %get-tuple-element.18.val, f32[64,256]{1,0:T(8,128)S(1)} %get-tuple-element.19.og, f32[256,256]{1,0:T(8,128)S(1)} %get-tuple-element.20.q, ...), custom_call_target="tpu_custom_call" | custom-call | tf_op jit(solution)/shard_map/cells/pallas_call | solution.py:437
  33.1 0.0 copy-done.1
  33.1 0.0 copy-done.2
  33.1 18.4 %readout.1 = (bf16[128,256]{1,0:T(8,128)(2,1)S(1)}, bf16[32,32,256]{2,1,0:T(8,128)(2,1)S(1)}) custom-call(bf16[64,256]{1,0:T(8,128)(2,1)S(1)} %get-tuple-element.24.gated, bf16[32,256]{1,0:T(8,128)(2,1)S(1)} %get-tuple-element.25.kown, bf16[128,2048]{1,0:T(8,128)(2,1)S(1)} %copy-done.1, bf16[128,256]{1,0:T(8,128)(2,1)S(1)} %copy-done.2), custom_call_target="tpu_custom_call" | custom-call | tf_op jit(solution)/shard_map/readout/pallas_call | solution.py:459
  51.5 1.2 %fusion = f32[1024,256]{1,0:T(8,128)} fusion(f32[1024,256]{1,0:T(8,128)S(1)} %copy-done, bf16[32,32,256]{2,1,0:T(8,128)(2,1)S(1)} %get-tuple-element.28, f32[4,256]{1,0:T(4,128)S(1)} %get-tuple-element.23.fre, f32[4,256]{1,0:T(4,128)S(1)} %get-tuple-element.22.dec), kind=kLoop, calls=%fused_computation.1 | loop fusion | flops 1048576 | bytes 2629632 | tf_op jit(solution)/shard_map/add | solution.py:482
  52.7 0.6 %copy.21 = bf16[128,256]{1,0:T(8,128)(2,1)} copy(bf16[128,256]{1,0:T(8,128)(2,1)S(1)} %get-tuple-element.34) | data formatting | bytes 131072
  53.3 0.6 %copy.22 = f32[4,256]{1,0:T(4,128)} copy(f32[4,256]{1,0:T(4,128)S(1)} %get-tuple-element.37) | data formatting | bytes 8192
Async XLA Ops:
  0.6 26.3 %copy-start = (f32[1024,256]{1,0:T(8,128)S(1)}, f32[1024,256]{1,0:T(8,128)}, u32[]{:S(2)}) copy-start(f32[1024,256]{1,0:T(8,128)} %norms.1) | copy-start | bytes 3145732
  0.6 32.4 %copy-start.1 = (bf16[128,2048]{1,0:T(8,128)(2,1)S(1)}, bf16[128,2048]{1,0:T(8,128)(2,1)}, u32[]{:S(2)}) copy-start(bf16[128,2048]{1,0:T(8,128)(2,1)} %w_read.1) | copy-start | bytes 1572868
  0.7 32.4 %copy-start.2 = (bf16[128,256]{1,0:T(8,128)(2,1)S(1)}, bf16[128,256]{1,0:T(8,128)(2,1)}, u32[]{:S(2)}) copy-start(bf16[128,256]{1,0:T(8,128)(2,1)} %tok.1) | copy-start | bytes 196612
